TPU v7x, 1024 devices: a whole 4x4x32 slice. The times are simulated.
1024 devices in a mesh: ep: 64 (over z, core), tp: 16 (over y, x).
Axes of the slice: x: 4, y: 4, z: 32, core: 2. Of those that a mesh axis runs over, the one named last changes fastest.
Arguments:
- tokens: bfloat16 [8192, 2048], P('ep'), may hold values from -6 to 6
- cotangent: bfloat16 [8192, 2048], P('ep'), may hold values from -1.796875 to 1.796875
- group_weight: float32 [8192], P('ep'), may hold values from 0.2 to 1
- expert_weight: float32 [8192, 2], P('ep'), may hold values from 0.1 to 0.9
- group_choice: int32 [8192], P('ep'), may hold values from 0 to 15, as said below
- local_choice: int32 [8192, 2], P('ep'), may hold values from 0 to 3, as said below
- w_gate: bfloat16 [64, 2048, 512], P('ep', None, 'tp'), may hold values from -0.125 to 0.125
- w_up: bfloat16 [64, 2048, 512], P('ep', None, 'tp'), may hold values from -0.125 to 0.125
- w_down: bfloat16 [64, 512, 2048], P('ep', 'tp'), may hold values from -0.25 to 0.25
Outputs:
- token_grad: float32 [8192, 2048], P('ep', 'tp')
- group_weight_grad: float32 [8192], P('ep')
- expert_weight_grad: float32 [8192, 2], P('ep')
- w_gate_grad: float32 [64, 2048, 512], P('ep', None, 'tp')
- w_up_grad: float32 [64, 2048, 512], P('ep', None, 'tp')
- w_down_grad: float32 [64, 512, 2048], P('ep', 'tp')
Inputs may be any that keep to these rules, and one draw needn't show every extreme that they name: Among the 128 tokens of each device (aligned blocks of tokens), no expert 4 * group_choice + local_choice is named by more than 6 slots, and some expert is named by exactly 6 slots of every device. `local_choice`: the 2 local choices of a token differ.
All inputs are finite; a program needn't handle non-finite values.
Results may differ from a plain program's by a relative error of at most 0.006.
Values may be sent and summed in bfloat16 or wider, within the bound.
A program may use at most 64 MiB of HBM per device.

v0:
```python
import jax
import jax.numpy as jnp
from jax import lax
from jax.sharding import Mesh
from jax.sharding import PartitionSpec as P

EPG = 4
TP = ("tp_0", "tp_1")


def in_one_piece(arrays, axis, split_dim, concat_dim, along):
    columns = [a.reshape(*a.shape[:along], -1) for a in arrays]
    both = jnp.concatenate(columns, axis=along)
    out, at, outs = (
        lax.all_to_all(both, axis, split_axis=split_dim, concat_axis=concat_dim, tiled=True),
        0,
        [],
    )
    for a, column in zip(arrays, columns):
        share = out[..., at : at + column.shape[along]]
        outs.append(share.reshape(*share.shape[:along], *a.shape[along:]))
        at += column.shape[along]
    return tuple(outs)


def sent_together(arrays, axis, dim, along):
    both = jnp.concatenate(arrays, axis=along)
    out, at, outs = (lax.all_gather(both, axis, axis=dim, tiled=True), 0, [])
    for a in arrays:
        outs.append(lax.slice_in_dim(out, at, at + a.shape[along], axis=along))
        at += a.shape[along]
    return tuple(outs)


def split_up(shard, dim, length):
    before, after = (shard.shape[:dim], shard.shape[dim + 1 :])
    return jnp.moveaxis(shard.reshape(*before, length, -1, *after), dim, 0)


def in_order(tiles, dim):
    tiles = jnp.moveaxis(tiles, 0, dim)
    shape = tiles.shape
    return tiles.reshape(*shape[:dim], shape[dim] * shape[dim + 1], *shape[dim + 2 :])


def moved_by_axis(tiles, axes, order):
    shape = [lax.axis_size(a) for a in axes]
    tiles = tiles.reshape(*shape, *tiles.shape[1:])
    for k in order:
        tiles = lax.all_to_all(tiles, axes[k], split_axis=k, concat_axis=k, tiled=True)
    return tiles.reshape(-1, *tiles.shape[len(axes) :])


def one_axis_at_a_time(shard, axes, order, split_dim, concat_dim):
    tiles = split_up(shard, split_dim, lax.axis_size(axes))
    return in_order(moved_by_axis(tiles, axes, order), concat_dim)


def turned_gather(arrays, axis, dims):
    turned = [jnp.moveaxis(a, dim, 0) for a, dim in zip(arrays, dims)]
    widths = [t[0].size for t in turned]
    both = jnp.concatenate([t.reshape(-1, w) for t, w in zip(turned, widths)], axis=1)
    out = lax.all_gather(both, axis, axis=0, tiled=True)
    tiles = jnp.split(out, [sum(widths[:k]) for k in range(1, len(widths))], axis=1)
    return tuple(
        (
            jnp.moveaxis(b.reshape(-1, *t.shape[1:]), 0, dim)
            for b, t, dim in zip(tiles, turned, dims)
        )
    )


def one_axis_at_a_time_2(shard, axes):
    for axis in axes:
        shard = lax.psum(shard, axis)
    return shard


def shards(
    tokens, cotangent, group_weight, expert_weight, group_choice, local_choice, w_gate, w_up, w_down
):
    token_count, feature_count = tokens.shape
    pick_count = expert_weight.shape[1]
    expert_count = lax.axis_size("ep")
    lane_count = lax.axis_size(TP)
    slot_count = token_count * pick_count
    capacity = pick_count * (3 * token_count // (2 * expert_count))
    buffer_count = expert_count * capacity
    piece_width = feature_count // lane_count
    expert_of = (group_choice[:, None] * EPG + local_choice).reshape(slot_count)
    member = (expert_of[:, None] == jnp.arange(expert_count, dtype=jnp.int32)[None, :]).astype(
        jnp.bfloat16
    )
    order = jnp.arange(slot_count, dtype=jnp.int32)
    earlier_mask = (order[:, None] > order[None, :]).astype(jnp.bfloat16)
    earlier = jnp.dot(earlier_mask, member, preferred_element_type=jnp.float32)
    position = jnp.sum(earlier * member.astype(jnp.float32), axis=1).astype(jnp.int32)
    slot_index = expert_of * capacity + position
    owner = (
        jnp.full((buffer_count,), token_count, jnp.int32).at[slot_index].set(order // pick_count)
    )
    gate_value = (group_weight[:, None] * expert_weight).astype(jnp.bfloat16).reshape(slot_count)
    gate_buffer = jnp.zeros((buffer_count,), jnp.bfloat16).at[slot_index].set(gate_value)
    start = lax.axis_index(TP) * piece_width
    token_cols = lax.dynamic_slice_in_dim(tokens, start, piece_width, 1)
    cot_cols = lax.dynamic_slice_in_dim(cotangent, start, piece_width, 1)
    token_part = jnp.take(token_cols, owner, axis=0, mode="fill", fill_value=0)
    cot_part = jnp.take(cot_cols, owner, axis=0, mode="fill", fill_value=0)
    token_part, gate_rows, cot_part = in_one_piece(
        (token_part, gate_buffer, cot_part), "ep", 0, 0, 1
    )
    arrived, cot_rows = sent_together((token_part, cot_part), TP, 1, 0)
    first = w_gate[0]
    second = w_up[0]
    third = w_down[0]
    contract_cols = (((1,), (1,)), ((), ()))
    contract_rows = (((0,), (0,)), ((), ()))
    pre_gate = jnp.dot(arrived, first, preferred_element_type=jnp.float32)
    pre_up = jnp.dot(arrived, second, preferred_element_type=jnp.float32)
    back_hidden = lax.dot_general(
        cot_rows, third, contract_cols, preferred_element_type=jnp.float32
    )
    sigma = jax.nn.sigmoid(pre_gate)
    swish = pre_gate * sigma
    hidden = swish * pre_up
    gate_part = jnp.sum(hidden * back_hidden, axis=1)
    gate_float = gate_rows.reshape(buffer_count, 1).astype(jnp.float32)
    scaled = gate_float * back_hidden
    grad_gate_pre = (scaled * pre_up * sigma * (1.0 + pre_gate * (1.0 - sigma))).astype(
        jnp.bfloat16
    )
    grad_up_pre = (scaled * swish).astype(jnp.bfloat16)
    weighted = (gate_float * hidden).astype(jnp.bfloat16)
    first_grad = lax.dot_general(
        arrived, grad_gate_pre, contract_rows, preferred_element_type=jnp.float32
    )
    second_grad = lax.dot_general(
        arrived, grad_up_pre, contract_rows, preferred_element_type=jnp.float32
    )
    third_grad = lax.dot_general(
        weighted, cot_rows, contract_rows, preferred_element_type=jnp.float32
    )
    first_rows, second_rows = (
        one_axis_at_a_time(first, TP, (0, 1), 0, 1),
        one_axis_at_a_time(second, TP, (0, 1), 0, 1),
    )
    pieces = turned_gather((grad_gate_pre, grad_up_pre), TP, (1, 1))
    total = lax.dot_general(
        pieces[0], first_rows, contract_cols, preferred_element_type=jnp.float32
    )
    summed = total + lax.dot_general(
        pieces[1], second_rows, contract_cols, preferred_element_type=jnp.float32
    )
    row_grad = summed.astype(jnp.bfloat16)
    gate_total = one_axis_at_a_time_2(gate_part, TP).astype(jnp.bfloat16)
    returned, gate_back = in_one_piece((row_grad, gate_total), "ep", 0, 0, 1)
    slot_grad = jnp.take(returned, slot_index, axis=0).astype(jnp.float32)
    token_grad = jnp.sum(slot_grad.reshape(token_count, pick_count, piece_width), axis=1)
    gate_grad = (
        jnp.take(gate_back, slot_index, axis=0).astype(jnp.float32).reshape(token_count, pick_count)
    )
    group_grad = jnp.sum(expert_weight * gate_grad, axis=1)
    expert_grad = group_weight[:, None] * gate_grad
    return (
        token_grad,
        group_grad,
        expert_grad,
        first_grad[None],
        second_grad[None],
        third_grad[None],
    )


def solution(mesh):
    split = Mesh(mesh.devices.reshape(mesh.shape["ep"], 4, 4), ("ep", "tp_0", "tp_1"))
    in_specs = (
        P("ep", None),
        P("ep", None),
        P("ep"),
        P("ep", None),
        P("ep"),
        P("ep", None),
        P("ep", None, TP),
        P("ep", None, TP),
        P("ep", TP, None),
    )
    out_specs = (
        P("ep", TP),
        P("ep"),
        P("ep", None),
        P("ep", None, TP),
        P("ep", None, TP),
        P("ep", TP, None),
    )
    return jax.shard_map(
        shards, mesh=split, in_specs=in_specs, out_specs=out_specs, check_vma=False
    )
```

profile of v0, /device:TPU:1, one launch (start us, length us, event | category | flops | bytes accessed | tf_op | source)
XLA Modules:
  0.0 293.1 jit_solution(6548125563633219823)
XLA Ops:
  11.6 1.4 gather_fusion.3
  13.0 1.4 gather_fusion.2
  15.0 2.2 scatter_custom_fusion.1
  17.6 83.4 %all_to_all.38 = bf16[64,6,257]{2,1,0:T(8,128)(2,1)S(1)} all-to-all(bf16[64,6,257]{2,1,0:T(8,128)(2,1)S(1)} %pad_maximum_fusion), channel_id=1, replica_groups=mesh['ep'=64,'tp_0'=4,'tp_1'=4] {'ep'}, dimensions={0} | all-to-all | bytes 394752 | tf_op jit(solution)/shard_map/all_to_all | solution.py:15
  102.8 4.2 %all-to-all-start.1 = ((bf16[4,4,128,32]{2,1,3,0:T(4,128)(2,1)}), bf16[4,4,128,32]{2,1,3,0:T(4,128)(2,1)S(1)}, u32[]{:S(2)}, u32[]{:S(2)}) async-start(bf16[4,4,128,32]{2,1,3,0:T(4,128)(2,1)} %copy.49), calls=%async_computation.1 | async-start | bytes 262144 | tf_op jit(solution)/shard_map/all_to_all | solution.py:50
  107.8 4.0 %all-to-all-done.1 = bf16[4,4,128,32]{2,1,3,0:T(4,128)(2,1)S(1)} async-done(((bf16[4,4,128,32]{2,1,3,0:T(4,128)(2,1)}), bf16[4,4,128,32]{2,1,3,0:T(4,128)(2,1)S(1)}, u32[]{:S(2)}, u32[]{:S(2)}) %all-to-all-start.1) | async-done | bytes 131104 | tf_op jit(solution)/shard_map/all_to_all | solution.py:50
  111.8 3.3 %all-to-all-start.3 = ((bf16[4,4,128,32]{2,1,3,0:T(4,128)(2,1)}), bf16[4,4,128,32]{2,1,3,0:T(4,128)(2,1)S(1)}, u32[]{:S(2)}, u32[]{:S(2)}) async-start(bf16[4,4,128,32]{2,1,3,0:T(4,128)(2,1)} %copy.52), calls=%async_computation.3 | async-start | bytes 262144 | tf_op jit(solution)/shard_map/all_to_all | solution.py:50
  115.8 4.1 %all-to-all-done.3 = bf16[4,4,128,32]{2,1,3,0:T(4,128)(2,1)S(1)} async-done(((bf16[4,4,128,32]{2,1,3,0:T(4,128)(2,1)}), bf16[4,4,128,32]{2,1,3,0:T(4,128)(2,1)S(1)}, u32[]{:S(2)}, u32[]{:S(2)}) %all-to-all-start.3) | async-done | bytes 131104 | tf_op jit(solution)/shard_map/all_to_all | solution.py:50
  120.0 4.7 %all-to-all-start.2 = ((bf16[4,4,128,32]{2,3,0,1:T(8,128)(2,1)}), bf16[4,4,128,32]{2,3,0,1:T(8,128)(2,1)S(1)}, u32[]{:S(2)}, u32[]{:S(2)}) async-start(bf16[4,4,128,32]{2,3,0,1:T(8,128)(2,1)} %copy.50), calls=%async_computation.2 | async-start | bytes 262144 | tf_op jit(solution)/shard_map/all_to_all | solution.py:50
  125.4 4.2 %all-to-all-done.2 = bf16[4,4,128,32]{2,3,0,1:T(8,128)(2,1)S(1)} async-done(((bf16[4,4,128,32]{2,3,0,1:T(8,128)(2,1)}), bf16[4,4,128,32]{2,3,0,1:T(8,128)(2,1)S(1)}, u32[]{:S(2)}, u32[]{:S(2)}) %all-to-all-start.2) | async-done | bytes 131104 | tf_op jit(solution)/shard_map/all_to_all | solution.py:50
  129.5 3.3 %all-to-all-start.4 = ((bf16[4,4,128,32]{2,3,0,1:T(8,128)(2,1)}), bf16[4,4,128,32]{2,3,0,1:T(8,128)(2,1)S(1)}, u32[]{:S(2)}, u32[]{:S(2)}) async-start(bf16[4,4,128,32]{2,3,0,1:T(8,128)(2,1)} %copy.53), calls=%async_computation.4 | async-start | bytes 262144 | tf_op jit(solution)/shard_map/all_to_all | solution.py:50
  132.9 4.8 %all-to-all-done.4 = bf16[4,4,128,32]{2,3,0,1:T(8,128)(2,1)S(1)} async-done(((bf16[4,4,128,32]{2,3,0,1:T(8,128)(2,1)}), bf16[4,4,128,32]{2,3,0,1:T(8,128)(2,1)S(1)}, u32[]{:S(2)}, u32[]{:S(2)}) %all-to-all-start.4) | async-done | bytes 131104 | tf_op jit(solution)/shard_map/all_to_all | solution.py:50
  137.8 32.8 %all-gather.2.cloned.1.call-done = bf16[768,2048]{1,0:T(8,128)(2,1)} async-done(((bf16[768,128]{1,0:T(8,128)(2,1)}), bf16[768,2048]{1,0:T(8,128)(2,1)}) %all-gather.2.cloned.1.call-update) | async-done | bytes 3145744 | tf_op jit(solution)/shard_map/all_gather | solution.py:28
  170.6 2.1 fusion.7
  172.7 2.0 fusion.9
  176.0 18.7 %all_gather.7 = bf16[512,768]{1,0:T(8,128)(2,1)S(1)} all-gather(bf16[32,768]{1,0:T(8,128)(2,1)S(1)} %pad_maximum_fusion.3), channel_id=1, replica_groups=mesh['ep'=64,'tp_0'=4,'tp_1'=4] {'tp_0','tp_1'}, dimensions={0}, use_global_device_ids=true | all-gather | bytes 835584 | tf_op jit(solution)/shard_map/all_gather | solution.py:63
  196.0 7.0 %psum.14 = f32[384]{0:T(512)S(1)} all-reduce(f32[384]{0:T(512)} %get-tuple-element.41), channel_id=1, replica_groups=mesh['ep'=64,'tp_0'=4,'tp_1'=4] {'tp_0'}, use_global_device_ids=true, to_apply=%region_4.6 | all-reduce | flops 384 | bytes 3072 | tf_op jit(solution)/shard_map/psum | solution.py:75
  203.0 8.1 %psum.15 = bf16[384]{0:T(512)(128)(2,1)S(1)} all-reduce(f32[384]{0:T(512)S(1)} %psum.14), channel_id=1, replica_groups=mesh['ep'=64,'tp_0'=4,'tp_1'=4] {'tp_1'}, use_global_device_ids=true, to_apply=%region_5.7 | all-reduce | flops 384 | bytes 2304 | tf_op jit(solution)/shard_map/psum | solution.py:75
  214.0 34.2 %all-to-all-start.5 = ((bf16[64,2,387]{2,1,0:T(2,128)(2,1)}), bf16[64,2,387]{2,1,0:T(2,128)(2,1)S(1)}, u32[]{:S(2)}, u32[]{:S(2)}) async-start(bf16[64,2,387]{2,1,0:T(2,128)(2,1)} %reshape.173), calls=%async_computation.5 | async-start | bytes 262144 | tf_op jit(solution)/shard_map/all_to_all | solution.py:15
  249.7 1.9 convolution_bitcast_fusion.2
  251.7 1.9 convolution_bitcast_fusion
  254.7 24.2 %all-to-all-done.5 = bf16[64,2,387]{2,1,0:T(2,128)(2,1)S(1)} async-done(((bf16[64,2,387]{2,1,0:T(2,128)(2,1)}), bf16[64,2,387]{2,1,0:T(2,128)(2,1)S(1)}, u32[]{:S(2)}, u32[]{:S(2)}) %all-to-all-start.5) | async-done | bytes 99104 | tf_op jit(solution)/shard_map/all_to_all | solution.py:15
  279.4 1.9 gather_fusion.1
  283.3 1.5 fusion.17
  (88 shorter events, 21.1 us)
Async XLA Ops:
  7.2 167.6 %copy-start = (bf16[1,32,2048]{2,1,0:T(8,128)(2,1)S(1)}, bf16[1,32,2048]{2,1,0:T(8,128)(2,1)}, u32[]{:S(2)}) copy-start(bf16[1,32,2048]{2,1,0:T(8,128)(2,1)} %param.19) | copy-start | bytes 393220
  7.2 7.5 %copy-start.13 = (f32[128]{0:T(128)S(1)}, f32[128]{0:T(128)}, u32[]{:S(2)}) copy-start(f32[128]{0:T(128)} %param.13) | copy-start | bytes 1540
  7.2 7.5 %copy-start.12 = (f32[128,2]{0,1:T(2,128)S(1)}, f32[128,2]{0,1:T(2,128)}, u32[]{:S(2)}) copy-start(f32[128,2]{0,1:T(2,128)} %param.14) | copy-start | bytes 3076
  7.2 163.4 %all-gather.2.cloned.1.call-start = ((), (), s32[]{:S(2)}) async-start(), calls=%async_computation.6 | async-start | bytes 3342336 | tf_op jit(solution)/shard_map/all_gather | solution.py:28
  8.8 2.0 copy-start.4
  9.3 92.7 %copy-start.10 = (bf16[1,2048,32]{1,2,0:T(8,128)(2,1)S(1)}, bf16[1,2048,32]{1,2,0:T(8,128)(2,1)}, u32[]{:S(2)}) copy-start(bf16[1,2048,32]{1,2,0:T(8,128)(2,1)} %param.17) | copy-start | bytes 393220
  13.0 94.0 %copy-start.11 = (bf16[1,2048,32]{1,2,0:T(8,128)(2,1)S(1)}, bf16[1,2048,32]{1,2,0:T(8,128)(2,1)}, u32[]{:S(2)}) copy-start(bf16[1,2048,32]{1,2,0:T(8,128)(2,1)} %param.18) | copy-start | bytes 393220
  102.8 9.0 %all-to-all-start.1 = ((bf16[4,4,128,32]{2,1,3,0:T(4,128)(2,1)}), bf16[4,4,128,32]{2,1,3,0:T(4,128)(2,1)S(1)}, u32[]{:S(2)}, u32[]{:S(2)}) async-start(bf16[4,4,128,32]{2,1,3,0:T(4,128)(2,1)} %copy.49), calls=%async_computation.1 | async-start | bytes 262144 | tf_op jit(solution)/shard_map/all_to_all | solution.py:50
  111.8 8.1 %all-to-all-start.3 = ((bf16[4,4,128,32]{2,1,3,0:T(4,128)(2,1)}), bf16[4,4,128,32]{2,1,3,0:T(4,128)(2,1)S(1)}, u32[]{:S(2)}, u32[]{:S(2)}) async-start(bf16[4,4,128,32]{2,1,3,0:T(4,128)(2,1)} %copy.52), calls=%async_computation.3 | async-start | bytes 262144 | tf_op jit(solution)/shard_map/all_to_all | solution.py:50
  120.0 9.6 %all-to-all-start.2 = ((bf16[4,4,128,32]{2,3,0,1:T(8,128)(2,1)}), bf16[4,4,128,32]{2,3,0,1:T(8,128)(2,1)S(1)}, u32[]{:S(2)}, u32[]{:S(2)}) async-start(bf16[4,4,128,32]{2,3,0,1:T(8,128)(2,1)} %copy.50), calls=%async_computation.2 | async-start | bytes 262144 | tf_op jit(solution)/shard_map/all_to_all | solution.py:50
  129.5 8.1 %all-to-all-start.4 = ((bf16[4,4,128,32]{2,3,0,1:T(8,128)(2,1)}), bf16[4,4,128,32]{2,3,0,1:T(8,128)(2,1)S(1)}, u32[]{:S(2)}, u32[]{:S(2)}) async-start(bf16[4,4,128,32]{2,3,0,1:T(8,128)(2,1)} %copy.53), calls=%async_computation.4 | async-start | bytes 262144 | tf_op jit(solution)/shard_map/all_to_all | solution.py:50
  170.6 4.2 %copy-start.1 = (bf16[768,2048]{1,0:T(8,128)(2,1)S(1)}, bf16[768,2048]{1,0:T(8,128)(2,1)}, u32[]{:S(2)}) copy-start(bf16[768,2048]{1,0:T(8,128)(2,1)} %all-gather.2.cloned.1.call-done) | copy-start | bytes 9437188
  172.7 22.3 %copy-start.2 = (f32[384,32]{0,1:T(8,128)}, f32[384,32]{0,1:T(8,128)S(1)}, u32[]{:S(2)}) copy-start(f32[384,32]{0,1:T(8,128)S(1)} %fusion.7) | copy-start | bytes 147460
  174.8 20.2 %copy-start.6 = (f32[384,32]{0,1:T(8,128)}, f32[384,32]{0,1:T(8,128)S(1)}, u32[]{:S(2)}) copy-start(f32[384,32]{0,1:T(8,128)S(1)} %fusion.9) | copy-start | bytes 147460
  175.9 19.1 %copy-start.8 = (f32[384,32]{0,1:T(8,128)}, f32[384,32]{0,1:T(8,128)S(1)}, u32[]{:S(2)}) copy-start(f32[384,32]{0,1:T(8,128)S(1)} %get-tuple-element.42) | copy-start | bytes 147460
  214.0 39.6 %copy-start.3 = (f32[384,32]{0,1:T(8,128)S(1)}, f32[384,32]{0,1:T(8,128)}, u32[]{:S(2)}) copy-start(f32[384,32]{0,1:T(8,128)} %copy-done.2) | copy-start | bytes 147460
  214.0 64.9 %all-to-all-start.5 = ((bf16[64,2,387]{2,1,0:T(2,128)(2,1)}), bf16[64,2,387]{2,1,0:T(2,128)(2,1)S(1)}, u32[]{:S(2)}, u32[]{:S(2)}) async-start(bf16[64,2,387]{2,1,0:T(2,128)(2,1)} %reshape.173), calls=%async_computation.5 | async-start | bytes 262144 | tf_op jit(solution)/shard_map/all_to_all | solution.py:15
  249.7 3.9 %copy-start.7 = (f32[384,32]{0,1:T(8,128)S(1)}, f32[384,32]{0,1:T(8,128)}, u32[]{:S(2)}) copy-start(f32[384,32]{0,1:T(8,128)} %copy-done.6) | copy-start | bytes 147460
  249.7 3.9 %copy-start.9 = (f32[384,32]{0,1:T(8,128)S(1)}, f32[384,32]{0,1:T(8,128)}, u32[]{:S(2)}) copy-start(f32[384,32]{0,1:T(8,128)} %copy-done.8) | copy-start | bytes 147460
  251.7 30.7 %copy-start.5 = (s32[128,2]{1,0:T(8,128)S(1)}, s32[128,2]{1,0:T(8,128)}, u32[]{:S(2)}) copy-start(s32[128,2]{1,0:T(8,128)} %copy-done.4) | copy-start | bytes 3076
  251.7 30.7 %copy-start.14 = (f32[128]{0:T(128)S(1)}, f32[128]{0:T(128)}, u32[]{:S(2)}) copy-start(f32[128]{0:T(128)} %param.13) | copy-start | bytes 1540
Sparse Core Ops, SparseCore 0:
  102.2 68.3 all-gather.1
where the time goes:
time: 294 us; the launch traced here: 293 us
  blocking collectives  117 us (40%)
  waiting for transfers between devices  74.1 us (25%)
  starting transfers between devices  49.8 us (17%)
  local copies, waits for them, and re-layouts  20.3 us (7%)
  between operations  14.5 us (5%)
  matrix products  11.1 us (4%)
  other arithmetic  6.2 us (2%)
    all_to_all x1, blocking collectives, in_one_piece(): lax.all_to_all(both, axis, split_axis=split_dim, concat_axis=concat_dim,...  83.4 us
    all_to_all x1, starting transfers between devices, in_one_piece(): lax.all_to_all(both, axis, split_axis=split_dim, concat_axis=concat_dim,...  34.2 us
    all_gather x1, waiting for transfers between devices, sent_together(): out, at, outs = (lax.all_gather(both, axis, axis=dim, tiled=True), 0, [])  32.8 us
    all_to_all x1, waiting for transfers between devices, in_one_piece(): lax.all_to_all(both, axis, split_axis=split_dim, concat_axis=concat_dim,...  24.2 us
    all_gather x1, blocking collectives, turned_gather(): out = lax.all_gather(both, axis, axis=0, tiled=True)  18.7 us
    all_to_all x4, waiting for transfers between devices, moved_by_axis(): lax.all_to_all(tiles, axes[k], split_axis=k, concat_axis=k, tiled=True)  17.1 us
    all_to_all x4, starting transfers between devices, moved_by_axis(): lax.all_to_all(tiles, axes[k], split_axis=k, concat_axis=k, tiled=True)  15.6 us
    psum x2, blocking collectives, one_axis_at_a_time_2(): shard = lax.psum(shard, axis)  15.1 us
  transfers between devices with their start and end apart: 6, of which 6 were waited for; matrix products, arithmetic and copies ran while one was open for 3% of the time, Pallas kernels for 0%

commit v1 on v0

v1 whole, which is shorter than its diff:
```python
import functools

import jax
import jax.numpy as jnp
from jax import lax
from jax.experimental import pallas as pl
from jax.experimental.pallas import tpu as pltpu
from jax.sharding import Mesh
from jax.sharding import PartitionSpec as P

EPG = 4
CAP = 6
LANES = 128
MESH = pl.DeviceIdType.MESH
F32 = jnp.float32
BF16 = jnp.bfloat16
NN = (((1,), (0,)), ((), ()))
NT = (((1,), (1,)), ((), ()))
TN = (((0,), (0,)), ((), ()))


def dot(a, b, dims=NN):
    return lax.dot_general(a, b, dims, preferred_element_type=F32)


def iota(shape, dim):
    return lax.broadcasted_iota(jnp.int32, shape, dim)


def hot(mask):
    return jnp.where(mask, 1.0, 0.0).astype(BF16)


def sixth(v):
    return (v * 10923) >> 16


def body(
    nz,
    chunks,
    route_ref,
    tok_hbm,
    cot_hbm,
    wg_hbm,
    wu_hbm,
    wd_hbm,
    token_out,
    small_out,
    gate_out,
    up_out,
    down_out,
    tok_v,
    cot_v,
    w2,
    wd_in,
    wd_p,
    send,
    recv,
    gates,
    arr_t,
    arr_c,
    w_rows,
    pieces,
    parts,
    ret_send,
    ret_recv,
    load_sem,
    z_send,
    z_recv,
    w_send,
    w_recv,
    a_send,
    a_recv,
    p_send,
    p_recv,
    q_send,
    q_recv,
    r_send,
    r_recv,
):
    z, c = lax.axis_index("z"), lax.axis_index("c")
    y, x = lax.axis_index("y"), lax.axis_index("x")
    ep, j = z * 2 + c, y * 4 + x
    experts = 2 * nz
    slots = experts * CAP
    per = experts // chunks
    rows = per * CAP
    half = rows // 2

    def z_peer(i, sign):
        k = 1 + i // 2
        dz = ((k + 1) // 2) * (2 * (k % 2) - 1)
        return k, lax.rem(z + sign * dz + nz, nz), lax.rem(i, 2)

    def plane_peer(i):
        p = lax.rem(j + i, 16)
        return p, {"y": p // 4, "x": lax.rem(p, 4)}

    barrier = pltpu.get_barrier_semaphore()

    def greet_z(i, _):
        _k, zz, cc = z_peer(i, 1)
        pl.semaphore_signal(barrier, inc=1, device_id={"z": zz, "c": cc}, device_id_type=MESH)
        return 0

    def greet_plane(i, _):
        _p, where = plane_peer(i)
        pl.semaphore_signal(barrier, inc=1, device_id=where, device_id_type=MESH)
        return 0

    lax.fori_loop(0, 2 * (nz - 1), greet_z, 0)
    pl.semaphore_signal(barrier, inc=1, device_id={"c": 1 - c}, device_id_type=MESH)
    lax.fori_loop(1, 16, greet_plane, 0)

    own = pl.ds(pl.multiple_of(j * LANES, LANES), LANES)
    loads = (
        pltpu.make_async_copy(tok_hbm.at[:, own], tok_v, load_sem.at[0]),
        pltpu.make_async_copy(cot_hbm.at[:, own], cot_v, load_sem.at[1]),
        pltpu.make_async_copy(wg_hbm, w2.at[pl.ds(0, 32)], load_sem.at[2]),
        pltpu.make_async_copy(wu_hbm, w2.at[pl.ds(32, 32)], load_sem.at[3]),
        pltpu.make_async_copy(wd_hbm, wd_in, load_sem.at[4]),
    )
    for load in loads:
        load.start()

    e0, e1 = route_ref[0:1, :], route_ref[1:2, :]
    g0, g1 = route_ref[2:3, :], route_ref[3:4, :]
    group_w, ew0, ew1 = route_ref[4:5, :], route_ref[5:6, :], route_ref[6:7, :]
    count = e0.shape[1]
    before = hot(iota((count, count), 0) < iota((count, count), 1))

    def named(n_rows, shift):
        expert = (iota((n_rows, count), 0) >> shift).astype(F32)
        in0, in1 = e0 == expert, e1 == expert
        member = in0 | in1
        place = dot(hot(member), before)
        return in0, in1, member, place

    in0, in1, member, place = named(experts, 0)
    gate_of = jnp.where(in0, g0, 0.0) + jnp.where(in1, g1, 0.0)
    lane = iota((experts, LANES), 1)
    gate_block = jnp.zeros((experts, LANES), F32)
    for q in range(CAP):
        col = jnp.sum(jnp.where(member & (place == q), gate_of, 0.0), axis=1, keepdims=True)
        gate_block = jnp.where(lane == q, col, gate_block)
    _i0, _i1, member16, place16 = named(experts * 16, 4)
    within = (iota((experts * 16, count), 0) & 15).astype(F32)
    pick_t = hot(member16 & (place16 == within))
    pick_c = hot(member16 & (place16 == within - CAP))
    row_of = iota((experts * 16, experts), 0)
    pick_g = hot(
        ((row_of >> 4) == iota((experts * 16, experts), 1)) & ((row_of & 15) == 2 * CAP)
    )
    loads[0].wait()
    loads[1].wait()
    block = dot(pick_t, tok_v[...]) + dot(pick_c, cot_v[...])
    block = block + dot(pick_g, gate_block.astype(BF16))
    send[...] = block.astype(BF16).reshape(experts, 16, LANES)
    recv[pl.ds(c, 1)] = send[pl.ds(ep, 1)]
    loads[2].wait()
    loads[3].wait()
    loads[4].wait()

    pl.semaphore_wait(barrier, 2 * (nz - 1) + 1 + 15)

    def z_copy(i):
        k, zz, cc = z_peer(i, 1)
        return pltpu.make_async_remote_copy(
            src_ref=send.at[zz * 2 + cc],
            dst_ref=recv.at[2 * k + c],
            send_sem=z_send.at[2 * k + cc],
            recv_sem=z_recv.at[2 * k + c],
            device_id={"z": zz, "c": cc},
            device_id_type=MESH,
        )

    partner = pltpu.make_async_remote_copy(
        src_ref=send.at[z * 2 + 1 - c],
        dst_ref=recv.at[c],
        send_sem=z_send.at[0],
        recv_sem=z_recv.at[c],
        device_id={"c": 1 - c},
        device_id_type=MESH,
    )
    partner.start()
    lax.fori_loop(0, 2 * (nz - 1), lambda i, _: (z_copy(i).start(), 0)[1], 0)

    def w_copy(i):
        p, where = plane_peer(i)
        return pltpu.make_async_remote_copy(
            src_ref=w2.at[:, pl.ds(pl.multiple_of(p * LANES, LANES), LANES)],
            dst_ref=w_rows.at[j],
            send_sem=w_send.at[i],
            recv_sem=w_recv.at[j],
            device_id=where,
            device_id_type=MESH,
        )

    lax.fori_loop(1, 16, lambda i, _: (w_copy(i).start(), 0)[1], 0)
    w_rows[pl.ds(j, 1)] = w2[:, own].reshape(1, 64, LANES)
    for a in range(4):
        for b in range(4):
            wd_p[:, (4 * b + a) * LANES : (4 * b + a + 1) * LANES] = wd_in[
                :, (4 * a + b) * LANES : (4 * a + b + 1) * LANES
            ]

    def cols(v, u):
        return pl.ds(pl.multiple_of((4 * v + u) * LANES, LANES), LANES)

    def wide(v):
        return pl.ds(pl.multiple_of(v * 4 * LANES, 4 * LANES), 4 * LANES)

    def ring(which, chunk):
        arr, u, v, u_axis, v_axis = (
            (arr_t, x, y, "x", "y") if which == 0 else (arr_c, y, x, "y", "x")
        )
        first = chunk * rows
        full, low, high = (
            pl.ds(first, rows),
            pl.ds(first, half),
            pl.ds(first + half, half),
        )
        up, um, u2 = lax.rem(u + 1, 4), lax.rem(u + 3, 4), lax.rem(u + 2, 4)
        vp, vm, v2 = lax.rem(v + 1, 4), lax.rem(v + 3, 4), lax.rem(v + 2, 4)

        def copy(n, ref, axis, to):
            return pltpu.make_async_remote_copy(
                src_ref=ref,
                dst_ref=ref,
                send_sem=a_send.at[which, chunk, n],
                recv_sem=a_recv.at[which, chunk, n],
                device_id={axis: to},
                device_id_type=MESH,
            )

        def sent(n):
            ref = (
                arr.at[full, cols(v, u)],
                arr.at[full, cols(v, u)],
                arr.at[low, cols(v, um)],
                arr.at[high, cols(v, up)],
                arr.at[full, wide(v)],
                arr.at[full, wide(v)],
                arr.at[low, wide(vm)],
                arr.at[high, wide(vp)],
            )[n]
            to = (up, um, up, um, vp, vm, vp, vm)[n]
            return copy(n, ref, u_axis if n < 4 else v_axis, to)

        def landed(n):
            copy(
                n,
                (
                    arr.at[full, cols(v, um)],
                    arr.at[full, cols(v, up)],
                    arr.at[low, cols(v, u2)],
                    arr.at[high, cols(v, u2)],
                    arr.at[full, wide(vm)],
                    arr.at[full, wide(vp)],
                    arr.at[low, wide(v2)],
                    arr.at[high, wide(v2)],
                )[n],
                u_axis if n < 4 else v_axis,
                up if n < 4 else vp,
            ).wait_recv()

        return sent, landed

    def step(number, chunk):
        for which in range(2):
            sent, landed = ring(which, chunk)
            if number == 1:
                sent(0).start()
                sent(1).start()
            elif number == 2:
                landed(0)
                sent(2).start()
                landed(1)
                sent(3).start()
            elif number == 3:
                landed(2)
                landed(3)
                sent(4).start()
                sent(5).start()
            elif number == 4:
                landed(4)
                sent(6).start()
                landed(5)
                sent(7).start()
            else:
                landed(6)
                landed(7)

    def z_landed(slot):
        pltpu.make_async_remote_copy(
            src_ref=send.at[0],
            dst_ref=recv.at[slot],
            send_sem=z_send.at[0],
            recv_sem=z_recv.at[slot],
            device_id={"c": 1 - c},
            device_id_type=MESH,
        ).wait_recv()

    pack_rows = 2 * rows + per
    r_id, c_id = iota((pack_rows, per * 16), 0), iota((pack_rows, per * 16), 1)
    second = jnp.where(r_id >= rows, 1, 0)
    r_in = r_id - second * rows
    r_slot = sixth(r_in)
    wanted = r_slot * 16 + (r_in - r_slot * CAP) + second * CAP
    wanted = jnp.where(r_id >= 2 * rows, (r_id - 2 * rows) * 16 + 2 * CAP, wanted)
    pack = hot(c_id == wanted)

    def arrive(chunk):
        if chunk == 0:
            z_landed(1 - c)
        lax.fori_loop(
            chunk * per + (2 if chunk == 0 else 0),
            (chunk + 1) * per,
            lambda s, _: (z_landed(s), 0)[1],
            0,
        )
        got = recv[chunk * per : (chunk + 1) * per].reshape(per * 16, LANES)
        packed = dot(pack, got)
        at = pl.ds(chunk * rows, rows)
        arr_t[at, cols(y, x)] = packed[:rows].astype(BF16)
        arr_c[at, cols(x, y)] = packed[rows : 2 * rows].astype(BF16)
        gates[chunk * per : (chunk + 1) * per, :] = packed[2 * rows :]

    for chunk in range(chunks):
        arrive(chunk)
        step(1, chunk)
        if chunk:
            step(4, chunk - 1)
        step(2, chunk)
        if chunk:
            step(5, chunk - 1)
        step(3, chunk)
    step(4, chunks - 1)
    step(5, chunks - 1)

    lane_slot = sixth(iota((experts, slots), 1))
    of_slot = lane_slot == iota((experts, slots), 0)
    lane_q = iota((LANES, slots), 1)
    lane_q = lane_q - sixth(lane_q) * CAP
    spread = hot(lane_q == iota((LANES, slots), 0))
    gate_row = jnp.sum(
        jnp.where(of_slot, dot(gates[...].astype(BF16), spread), 0.0), axis=0, keepdims=True
    )
    pre = dot(w2[...], arr_t[...], NT)
    back = dot(wd_p[...], arr_c[...], NT)
    pre_gate, pre_up = pre[:32], pre[32:]
    sigma = jax.nn.sigmoid(pre_gate)
    swish = pre_gate * sigma
    hidden = swish * pre_up
    part = jnp.sum(hidden * back, axis=0, keepdims=True)
    scaled = gate_row * back
    grads = jnp.concatenate(
        [scaled * pre_up * sigma * (1.0 + pre_gate * (1.0 - sigma)), scaled * swish], axis=0
    ).astype(BF16)
    weighted = (gate_row * hidden).astype(BF16)
    pieces[pl.ds(j, 1)] = grads.reshape(1, 64, slots)
    parts[pl.ds(j, 1)] = part.reshape(1, 1, slots)

    def p_copy(i):
        _p, where = plane_peer(i)
        return pltpu.make_async_remote_copy(
            src_ref=pieces.at[j],
            dst_ref=pieces.at[j],
            send_sem=p_send.at[i],
            recv_sem=p_recv.at[j],
            device_id=where,
            device_id_type=MESH,
        )

    def q_copy(i):
        _p, where = plane_peer(i)
        return pltpu.make_async_remote_copy(
            src_ref=parts.at[j],
            dst_ref=parts.at[j],
            send_sem=q_send.at[i],
            recv_sem=q_recv.at[j],
            device_id=where,
            device_id_type=MESH,
        )

    def plane_landed(i):
        p, where = plane_peer(i)
        for ref, s_sem, r_sem in (
            (pieces, p_send, p_recv),
            (parts, q_send, q_recv),
            (w_rows, w_send, w_recv),
        ):
            pltpu.make_async_remote_copy(
                src_ref=ref.at[p],
                dst_ref=ref.at[p],
                send_sem=s_sem.at[i],
                recv_sem=r_sem.at[p],
                device_id=where,
                device_id_type=MESH,
            ).wait_recv()

    lax.fori_loop(1, 16, lambda i, _: (p_copy(i).start(), q_copy(i).start(), 0)[2], 0)
    lax.fori_loop(1, 16, lambda i, _: (plane_landed(i), 0)[1], 0)

    row_grad = dot(
        pieces[...].reshape(16 * 64, slots), w_rows[...].reshape(16 * 64, LANES), TN
    ).astype(BF16)
    total = jnp.sum(parts[...], axis=0).astype(BF16).astype(F32)
    held = dot(jnp.where(of_slot, total, 0.0).astype(BF16), spread, NT)
    r_id, c_id = iota((experts * 8, slots), 0), iota((experts * 8, slots), 1)
    unpack = hot((c_id == (r_id >> 3) * CAP + (r_id & 7)) & ((r_id & 7) < CAP))
    r_id, c_id = iota((experts * 8, experts), 0), iota((experts * 8, experts), 1)
    unheld = hot((c_id == (r_id >> 3)) & ((r_id & 7) == CAP))
    back_block = dot(unpack, row_grad) + dot(unheld, held.astype(BF16))
    ret_send[...] = back_block.astype(BF16).reshape(experts, 8, LANES)
    ret_recv[pl.ds(ep, 1)] = ret_send[pl.ds(c, 1)]

    def r_copy(i):
        k, zz, cc = z_peer(i, -1)
        return pltpu.make_async_remote_copy(
            src_ref=ret_send.at[2 * k + cc],
            dst_ref=ret_recv.at[ep],
            send_sem=r_send.at[2 * k + cc],
            recv_sem=r_recv.at[ep],
            device_id={"z": zz, "c": cc},
            device_id_type=MESH,
        )

    r_partner = pltpu.make_async_remote_copy(
        src_ref=ret_send.at[1 - c],
        dst_ref=ret_recv.at[ep],
        send_sem=r_send.at[0],
        recv_sem=r_recv.at[ep],
        device_id={"c": 1 - c},
        device_id_type=MESH,
    )
    lax.fori_loop(
        0, 2 * (nz - 1), lambda i, _: (r_copy(2 * (nz - 1) - 1 - i).start(), 0)[1], 0
    )
    r_partner.start()

    first_two = dot(grads, arr_t[...])
    gate_out[...] = first_two[:32]
    up_out[...] = first_two[32:]
    third = dot(weighted, arr_c[...])
    for a in range(4):
        for b in range(4):
            down_out[:, (4 * a + b) * LANES : (4 * a + b + 1) * LANES] = third[
                :, (4 * b + a) * LANES : (4 * b + a + 1) * LANES
            ]

    def r_landed(i):
        e = lax.rem(ep + i, experts)
        pltpu.make_async_remote_copy(
            src_ref=ret_send.at[0],
            dst_ref=ret_recv.at[e],
            send_sem=r_send.at[0],
            recv_sem=r_recv.at[e],
            device_id={"c": 1 - c},
            device_id_type=MESH,
        ).wait_recv()

    lax.fori_loop(1, experts, lambda i, _: (r_landed(i), 0)[1], 0)

    returned = ret_recv[...].reshape(experts * 8, LANES)
    _i0, _i1, member8, place8 = named(experts * 8, 3)
    within = (iota((experts * 8, count), 0) & 7).astype(F32)
    token_out[...] = dot(hot(member8 & (place8 == within)), returned, TN)
    r_id, c_id = iota((experts, experts * 8), 0), iota((experts, experts * 8), 1)
    held_back = dot(hot(c_id == r_id * 8 + CAP), returned).astype(BF16)
    held_rows = []
    for inside in (in0, in1):
        spot = jnp.sum(jnp.where(inside, place, 0.0), axis=0, keepdims=True)
        mixed = dot(held_back, hot(inside), TN)
        at_spot = iota((LANES, count), 0).astype(F32) == spot
        held_rows.append(jnp.sum(jnp.where(at_spot, mixed, 0.0), axis=0, keepdims=True))
    small_out[0:1, :] = group_w * held_rows[0]
    small_out[1:2, :] = group_w * held_rows[1]
    small_out[2:3, :] = ew0 * held_rows[0] + ew1 * held_rows[1]
    small_out[3:8, :] = jnp.zeros((5, count), F32)

    partner.wait_send()
    lax.fori_loop(0, 2 * (nz - 1), lambda i, _: (z_copy(i).wait_send(), 0)[1], 0)
    r_partner.wait_send()
    lax.fori_loop(0, 2 * (nz - 1), lambda i, _: (r_copy(i).wait_send(), 0)[1], 0)

    def plane_left(i, _):
        w_copy(i).wait_send()
        p_copy(i).wait_send()
        q_copy(i).wait_send()
        return 0

    lax.fori_loop(1, 16, plane_left, 0)
    for chunk in range(chunks):
        for which in range(2):
            sent, _landed = ring(which, chunk)
            for n in range(8):
                sent(n).wait_send()


def run(nz, chunks, route, tokens, cotangent, wg, wu, wd):
    experts = 2 * nz
    slots = experts * CAP
    count, width = tokens.shape
    dma = pltpu.SemaphoreType.DMA
    hbm = pl.BlockSpec(memory_space=pl.ANY)
    vmem = pl.BlockSpec(memory_space=pltpu.VMEM)
    return pl.pallas_call(
        functools.partial(body, nz, chunks),
        out_shape=(
            jax.ShapeDtypeStruct((count, LANES), F32),
            jax.ShapeDtypeStruct((8, count), F32),
            jax.ShapeDtypeStruct((32, width), F32),
            jax.ShapeDtypeStruct((32, width), F32),
            jax.ShapeDtypeStruct((32, width), F32),
        ),
        in_specs=[vmem, hbm, hbm, hbm, hbm, hbm],
        out_specs=(vmem,) * 5,
        scratch_shapes=[
            pltpu.VMEM((count, LANES), BF16),
            pltpu.VMEM((count, LANES), BF16),
            pltpu.VMEM((64, width), BF16),
            pltpu.VMEM((32, width), BF16),
            pltpu.VMEM((32, width), BF16),
            pltpu.VMEM((experts, 16, LANES), BF16),
            pltpu.VMEM((experts, 16, LANES), BF16),
            pltpu.VMEM((experts, LANES), F32),
            pltpu.VMEM((slots, width), BF16),
            pltpu.VMEM((slots, width), BF16),
            pltpu.VMEM((16, 64, LANES), BF16),
            pltpu.VMEM((16, 64, slots), BF16),
            pltpu.VMEM((16, 1, slots), F32),
            pltpu.VMEM((experts, 8, LANES), BF16),
            pltpu.VMEM((experts, 8, LANES), BF16),
            dma((5,)),
            dma((experts,)),
            dma((experts,)),
            dma((16,)),
            dma((16,)),
            dma((2, chunks, 8)),
            dma((2, chunks, 8)),
            dma((16,)),
            dma((16,)),
            dma((16,)),
            dma((16,)),
            dma((experts,)),
            dma((experts,)),
        ],
        compiler_params=pltpu.CompilerParams(collective_id=0, has_side_effects=True),
        name="experts",
    )(route, tokens, cotangent, wg, wu, wd)


def shards(
    nz,
    chunks,
    tokens,
    cotangent,
    group_weight,
    expert_weight,
    group_choice,
    local_choice,
    w_gate,
    w_up,
    w_down,
):
    ids = (group_choice[None, :] * EPG + local_choice.T).astype(F32)
    gate = (group_weight[None, :] * expert_weight.T).astype(BF16).astype(F32)
    zero = jnp.zeros((1, tokens.shape[0]), F32)
    route = jnp.concatenate([ids, gate, group_weight[None, :], expert_weight.T, zero], axis=0)
    token_grad, small, gate_grad, up_grad, down_grad = run(
        nz,
        chunks,
        route,
        tokens,
        cotangent,
        w_gate[0].T,
        w_up[0].T,
        w_down[0],
    )
    return (
        token_grad,
        small[2],
        small[0:2].T,
        gate_grad.T[None],
        up_grad.T[None],
        down_grad[None],
    )


def build(mesh, chunks):
    nz = mesh.shape["ep"] // 2
    split = Mesh(mesh.devices.reshape(nz, 2, 4, 4), ("z", "c", "y", "x"))
    ep, tp = ("z", "c"), ("y", "x")
    in_specs = (
        P(ep, None),
        P(ep, None),
        P(ep),
        P(ep, None),
        P(ep),
        P(ep, None),
        P(ep, None, tp),
        P(ep, None, tp),
        P(ep, tp, None),
    )
    out_specs = (
        P(ep, tp),
        P(ep),
        P(ep, None),
        P(ep, None, tp),
        P(ep, None, tp),
        P(ep, tp, None),
    )
    return jax.shard_map(
        functools.partial(shards, nz, chunks),
        mesh=split,
        in_specs=in_specs,
        out_specs=out_specs,
        check_vma=False,
    )


def solution(mesh):
    return build(mesh, 4)
```

time: 294 us -> 126 us (0.43)
  blocking collectives: 117 us -> 0 us
  Pallas kernels: 0 us -> 115 us
  waiting for transfers between devices: 74.1 us -> 0 us
  starting transfers between devices: 49.8 us -> 0 us
  between operations: 14.5 us -> 0.66 us
  local copies, waits for them, and re-layouts: 20.3 us -> 8.65 us
  matrix products: 11.1 us -> 0 us
  other arithmetic: 6.2 us -> 0.67 us
    pallas_call x0 -> x1, Pallas kernels: none -> 115 us  [run(): pl.pallas_call(functools.partial(body, nz, chunks), out_shape=(jax.ShapeD...]
    all_to_all x1 -> x0, blocking collectives: 83.4 us -> none  [in_one_piece(): lax.all_to_all(both, axis, split_axis=split_dim, concat_axis=concat_dim,...]
    all_to_all x5 -> x0, starting transfers between devices: 49.8 us -> none  [the longest x1 34.2 us: in_one_piece(): lax.all_to_all(both, axis, split_axis=split_dim, concat_axis=concat_dim,...]
    all_to_all x5 -> x0, waiting for transfers between devices: 41.3 us -> none  [the longest x1 24.2 us: in_one_piece(): lax.all_to_all(both, axis, split_axis=split_dim, concat_axis=concat_dim,...]
    all_gather x1 -> x0, waiting for transfers between devices: 32.8 us -> none  [sent_together(): out, at, outs = (lax.all_gather(both, axis, axis=dim, tiled=True), 0, [])]
    all_gather x1 -> x0, blocking collectives: 18.7 us -> none  [turned_gather(): out = lax.all_gather(both, axis, axis=0, tiled=True)]
    psum x2 -> x0, blocking collectives: 15.1 us -> none  [one_axis_at_a_time_2(): shard = lax.psum(shard, axis)]
    dot_general x9 -> x0, matrix products: 11.1 us -> none  [the longest x1 2.12 us: shards(): pre_gate = jnp.dot(arrived, first, preferred_element_type=jnp.float32)]
  transfers between devices with their start and end apart: 6 -> 0, of which waited for: 6 -> 0; matrix products, arithmetic and copies ran while one was open for 3% -> 0% of each run, Pallas kernels for 0% -> 0%
where the time goes in v1:
time: 126 us; the launch traced here: 125 us
  Pallas kernels  115 us (91%)
  local copies, waits for them, and re-layouts  8.65 us (7%)
    pallas_call x1, Pallas kernels, run(): pl.pallas_call(functools.partial(body, nz, chunks), out_shape=(jax.ShapeD...  115 us
    unnamed x14, local copies, waits for them, and re-layouts  5.62 us

profile of v1, /device:TPU:1, one launch (start us, length us, event | category | flops | bytes accessed | tf_op | source)
XLA Modules:
  0.0 125.3 jit_solution(7774199049976759312)
XLA Ops:
  0.6 0.0 copy-start.4
  0.6 0.7 broadcast_multiply_fusion
  1.3 0.0 copy-done.4
  1.3 0.0 copy-start.2
  1.3 0.0 copy-start.3
  1.3 0.7 copy-done.2
  2.0 0.0 copy-done.3
  2.0 0.6 concatenate.3.route_ref
  2.6 115.3 %experts.1 = (f32[128,128]{1,0:T(8,128)}, f32[8,128]{1,0:T(8,128)}, f32[32,2048]{1,0:T(8,128)}, f32[32,2048]{1,0:T(8,128)}, f32[32,2048]{1,0:T(8,128)}) custom-call(f32[8,128]{1,0:T(8,128)} %concatenate.3.route_ref, bf16[128,2048]{1,0:T(8,128)(2,1)} %tok_hbm.1, bf16[128,2048]{1,0:T(8,128)(2,1)} %cot_hbm.1, bf16[32,2048]{1,0:T(8,128)(2,1)} %bitcast.26, ...), custom_call_target="tpu_custom_call" | custom-call | tf_op jit(solution)/shard_map/experts/pallas_call | solution.py:508
  117.9 1.2 slice_bitcast_fusion
  119.1 1.2 slice_bitcast_fusion.1
  120.3 1.5 %copy.19 = f32[128,128]{1,0:T(8,128)} copy(f32[128,128]{1,0:T(8,128)} %get-tuple-element.22) | data formatting | bytes 131072
  121.8 0.0 copy-start.1
  121.8 1.7 %copy.20 = f32[1,2048,32]{1,2,0:T(8,128)} copy(f32[1,2048,32]{1,2,0:T(8,128)} %bitcast.25) | data formatting | bytes 524288
  123.5 0.0 copy-done.1
  123.5 0.0 copy-start
  123.5 0.7 copy.21
  124.2 0.3 copy-done
  124.6 0.7 copy.22
  (3 shorter events, 0.0 us)
Async XLA Ops:
  0.6 0.7 copy-start.4
  1.3 0.7 copy-start.2
  1.3 0.7 copy-start.3
  121.8 1.7 %copy-start.1 = (f32[32,2048]{1,0:T(8,128)S(1)}, f32[32,2048]{1,0:T(8,128)}, u32[]{:S(2)}) copy-start(f32[32,2048]{1,0:T(8,128)} %get-tuple-element.14) | copy-start | bytes 786436
  123.5 1.0 copy-start
